TPU v7x, 32 devices: a whole 2x2x4 slice. The times are simulated.
32 devices in a mesh: grp: 2 (over y), fs: 4 (over z), tp: 4 (over x, core).
Axes of the slice: x: 2, y: 2, z: 4, core: 2. Of those that a mesh axis runs over, the one named last changes fastest.
Arguments:
- tokens: bfloat16 [512, 2048], P(('grp', 'fs')), parts along dimension 0, may hold values from -6 to 6
- routes: int32 [512, 2], P(('grp', 'fs')), parts along dimension 0, may hold values from 0 to 3, as said below
- route_logits: float32 [512, 2], P(('grp', 'fs')), parts along dimension 0, may hold values from -8 to 8
- gain: float32 [2048], P('fs'), may hold values from 0.1 to 1.9
- w_gate: float32 [4, 2048, 7168], P(None, 'fs', 'tp'), may hold values from -0.125 to 0.125
- w_up: float32 [4, 2048, 7168], P(None, 'fs', 'tp'), may hold values from -0.125 to 0.125
- w_down: float32 [4, 7168, 2048], P(None, 'fs', 'tp'), may hold values from -0.0625 to 0.0625
Outputs:
- gate_served: bfloat16 [8, 2048, 7168], P(('grp', 'tp'), None, 'fs'), parts along dimension 0
- up_served: bfloat16 [8, 2048, 7168], P(('grp', 'tp'), None, 'fs'), parts along dimension 0
- down_served: bfloat16 [8, 7168, 2048], P(('grp', 'tp'), 'fs'), parts along dimension 0
- mixed: bfloat16 [512, 2048], P(('grp', 'fs'), 'tp'), parts along dimension 0
There are 2 independent parts, one for each index of `grp`. A program takes and returns all parts, laid end to end along the dimension named above; an argument that names none is the same for every part. Nothing has to cross between parts.
Inputs may be any that keep to these rules, and one draw needn't show every extreme that they name: `routes`: each row names 2 different experts; every expert is named by some row.
All inputs are finite; a program needn't handle non-finite values.
Results may differ from a plain program's by a relative error of at most 0.0085.
Values may be sent and summed in bfloat16 or wider, within the bound.
A program may use at most 192 MiB of HBM per device.

v0:
```python
import functools

import jax
import jax.numpy as jnp
from jax import lax
from jax.experimental import pallas as pl
from jax.experimental.pallas import tpu as pltpu
from jax.sharding import PartitionSpec as P

BF16 = jnp.bfloat16
F32 = jnp.float32
CHUNKS = 4
DOWN_CHUNKS = 4
LAGS = (2, 3, 4)
LOADS = 4


def move_kernel(
    groups, n, gain_ref, wg_ref, wu_ref, wd_ref, og_ref, ou_ref, od_ref,
    wide, wide_d, stage, extra, relay, stage_d,
    load_sem, s1s, s1r, xs, xr, zs, zr, ys, yr, ds, dr,
):
    g, f, t = lax.axis_index("grp"), lax.axis_index("fs"), lax.axis_index("tp")
    rows = wg_ref.shape[1]
    half = rows // groups
    ch = half // CHUNKS
    hidden, width = wd_ref.shape[1:]
    dh = hidden // DOWN_CHUNKS
    weights, outs = (wg_ref, wu_ref), (og_ref, ou_ref)
    items = 2 * CHUNKS

    mate = t + 1 - 2 * lax.rem(t, 2)
    peers = (t, mate, lax.rem(t + 2, n), lax.rem(mate + 2, n))
    home = f == t

    def remote(src, dst, ssem, rsem, where):
        return pltpu.make_async_remote_copy(
            src_ref=src, dst_ref=dst, send_sem=ssem, recv_sem=rsem,
            device_id=where, device_id_type=pl.DeviceIdType.MESH,
        )

    barrier = pltpu.get_barrier_semaphore()
    for k in (1, 2, 3):
        pl.semaphore_signal(barrier, inc=1, device_id=(g, f, peers[k]), device_id_type=pl.DeviceIdType.MESH)
    for d in range(1, n):
        pl.semaphore_signal(barrier, inc=1, device_id=(g, lax.rem(f + d, n), t), device_id_type=pl.DeviceIdType.MESH)
    pl.semaphore_signal(barrier, inc=1, device_id=(1 - g, f, t), device_id_type=pl.DeviceIdType.MESH)
    pl.semaphore_wait(barrier, 2 * n - 1)

    def own_row(c):
        return pl.multiple_of(g * half + c * ch, ch)

    def other_row(c):
        return pl.multiple_of((1 - g) * half + c * ch, ch)

    def at_rows(u, source, row):
        return outs[u].at[pl.ds(pl.multiple_of(source * rows + row, ch), ch), :]

    def first(k, u, c):
        return remote(stage.at[k, u, c], relay.at[k - 1, u, c], s1s.at[k, u, c], s1r.at[k, u, c], (g, f, peers[k]))

    def first_home(k, u, c):
        return remote(stage.at[k, u, c], at_rows(u, f, own_row(c)), s1s.at[k, u, c], s1r.at[k, u, c], (g, f, peers[k]))

    def own_home(u, c):
        return pltpu.make_async_copy(stage.at[0, u, c], at_rows(u, f, own_row(c)), s1s.at[0, u, c])

    def extra_home(u, c):
        return pltpu.make_async_copy(extra.at[0, u, c], at_rows(u, f, other_row(c)), xs.at[0, u, c])

    def extra_mate(u, c):
        return remote(extra.at[1, u, c], at_rows(u, f, other_row(c)), xs.at[1, u, c], xr.at[u, c], (g, f, mate))

    def layer(k, u, c):
        src = stage.at[0, u, c] if k == 0 else relay.at[k - 1, u, c]
        return remote(src, at_rows(u, f, own_row(c)), zs.at[k, u, c], zr.at[f, u, c], (g, peers[k], t))

    def layer_in(source, u, c):
        piece = at_rows(u, source, own_row(c))
        return remote(piece, piece, zs.at[0, u, c], zr.at[source, u, c], (1 - g, f, t))

    def across(source, u, c):
        piece = at_rows(u, source, own_row(c))
        return remote(piece, piece, ys.at[source, u, c], yr.at[source, u, c], (1 - g, f, t))

    def down(k, c):
        src = stage_d.at[k, c]
        dst = od_ref.at[pl.ds(c * dh, dh), pl.ds(pl.multiple_of(t * width, 128), width)]
        if k == 0:
            return pltpu.make_async_copy(src, dst, ds.at[0, c])
        return remote(src, dst, ds.at[k, c], dr.at[k, c], (g, f, peers[k]))

    order = (2, 0, 3, 1)

    def load(u, k, row, slot):
        return pltpu.make_async_copy(weights[u].at[peers[k], pl.ds(row, ch), :], wide.at[slot], load_sem.at[slot])

    def load_d(k, c, slot):
        return pltpu.make_async_copy(wd_ref.at[peers[k], pl.ds(c * dh, dh), :], wide_d.at[slot], load_sem.at[LOADS + slot])

    def fold(slot, row, dst):
        scale = gain_ref[pl.ds(row, ch), :]
        dst[...] = (wide[slot] * scale).astype(BF16)

    for j, k in enumerate(order):
        load(0, k, own_row(0), j).start()
    for u in range(2):
        def trip(c, _, u=u):
            for j, k in enumerate(order):
                load(u, k, own_row(c), j).wait()
                fold(j, own_row(c), stage.at[k, u, c])

                @pl.when(c < CHUNKS - 1)
                def _():
                    load(u, k, own_row(c + 1), j).start()

                if u == 0:
                    @pl.when(c == CHUNKS - 1)
                    def _():
                        load(1, k, own_row(0), j).start()

                if k == 0:
                    @pl.when(home)
                    def _():
                        own_home(u, c).start()

                    @pl.when(jnp.logical_not(home))
                    def _():
                        layer(0, u, c).start()
                else:
                    @pl.when(home)
                    def _():
                        first_home(k, u, c).start()

                    @pl.when(jnp.logical_not(home))
                    def _():
                        first(k, u, c).start()
            return 0

        lax.fori_loop(0, CHUNKS, trip, 0)

    for j, k in enumerate(order):
        load_d(k, 0, j).start()

    def trip_d(c, _):
        for j, k in enumerate(order):
            load_d(k, c, j).wait()
            stage_d[k, c] = wide_d[j].astype(BF16)

            @pl.when(c < DOWN_CHUNKS - 1)
            def _():
                load_d(k, c + 1, j).start()

            down(k, c).start()
        return 0

    lax.fori_loop(0, DOWN_CHUNKS, trip_d, 0)

    @pl.when(home)
    def _():
        for u in range(2):
            def trip_x(c, _, u=u):
                for k in (0, 1):
                    copy = load(u, k, other_row(c), k)
                    copy.start()
                    copy.wait()
                    fold(k, other_row(c), extra.at[k, u, c])
                    (extra_home if k == 0 else extra_mate)(u, c).start()
                return 0

            lax.fori_loop(0, CHUNKS, trip_x, 0)

    def forward_z(k, u, c):
        away = peers[k] != f

        @pl.when(away)
        def _():
            first(k, u, c).wait_recv()
            layer(k, u, c).start()

        @pl.when(jnp.logical_not(away))
        def _():
            first_home(k, u, c).wait_recv()
            if k >= 2:
                across(f, u, c).start()

    def forward_y(d, u, c):
        for sign in (1, -1):
            source = f + sign * d

            @pl.when((source >= 0) & (source < n))
            def _():
                layer_in(source, u, c).wait_recv()
                across(source, u, c).start()

    def at_item(fn, i):
        u, c = i // CHUNKS, lax.rem(i, CHUNKS)
        for v in range(2):
            @pl.when(u == v)
            def _():
                fn(v, c)

    def trip_f(i, _):
        def z_part(u, c):
            for k in (1, 2, 3):
                forward_z(k, u, c)

        @pl.when(i < items)
        def _():
            at_item(z_part, i)

        for d in range(1, n):
            lag = LAGS[d - 1]

            @pl.when((i >= lag) & (i < items + lag))
            def _():
                at_item(functools.partial(forward_y, d), i - lag)

        return 0

    lax.fori_loop(0, items + max(LAGS), trip_f, 0)

    for u in range(2):
        def trip_w(c, _, u=u):
            @pl.when(home)
            def _():
                own_home(u, c).wait()
                extra_home(u, c).wait()
                extra_mate(u, c).wait_send()

            @pl.when(jnp.logical_not(home))
            def _():
                layer(0, u, c).wait_send()

            @pl.when(f == mate)
            def _():
                extra_mate(u, c).wait_recv()

            for k in (1, 2, 3):
                first(k, u, c).wait_send()

                @pl.when(peers[k] != f)
                def _():
                    layer(k, u, c).wait_send()

                if k >= 2:
                    @pl.when(peers[k] == f)
                    def _():
                        across(f, u, c).wait()

            for d in range(1, n):
                for sign in (1, -1):
                    source = f + sign * d

                    @pl.when((source >= 0) & (source < n))
                    def _():
                        across(source, u, c).wait()
            return 0

        lax.fori_loop(0, CHUNKS, trip_w, 0)

    def trip_wd(c, _):
        for k in range(n):
            down(k, c).wait()
        return 0

    lax.fori_loop(0, DOWN_CHUNKS, trip_wd, 0)


def move(groups, n, gain, w_gate, w_up, w_down):
    experts, rows, cols = w_gate.shape
    hidden, width = w_down.shape[1:]
    ch = rows // groups // CHUNKS
    dh = hidden // DOWN_CHUNKS
    dma = pltpu.SemaphoreType.DMA
    hbm = pl.BlockSpec(memory_space=pl.ANY)
    return pl.pallas_call(
        functools.partial(move_kernel, groups, n),
        out_shape=(
            jax.ShapeDtypeStruct((rows * n, cols), BF16),
            jax.ShapeDtypeStruct((rows * n, cols), BF16),
            jax.ShapeDtypeStruct((hidden, width * n), BF16),
        ),
        in_specs=[pl.BlockSpec(memory_space=pltpu.VMEM), hbm, hbm, hbm],
        out_specs=(hbm, hbm, hbm),
        scratch_shapes=[
            pltpu.VMEM((LOADS, ch, cols), F32),
            pltpu.VMEM((LOADS, dh, width), F32),
            pltpu.VMEM((n, 2, CHUNKS, ch, cols), BF16),
            pltpu.VMEM((2, 2, CHUNKS, ch, cols), BF16),
            pltpu.VMEM((n - 1, 2, CHUNKS, ch, cols), BF16),
            pltpu.VMEM((n, DOWN_CHUNKS, dh, width), BF16),
            dma((2 * LOADS,)),
            dma((n, 2, CHUNKS)),
            dma((n, 2, CHUNKS)),
            dma((2, 2, CHUNKS)),
            dma((2, CHUNKS)),
            dma((n, 2, CHUNKS)),
            dma((n, 2, CHUNKS)),
            dma((n, 2, CHUNKS)),
            dma((n, 2, CHUNKS)),
            dma((n, DOWN_CHUNKS)),
            dma((n, DOWN_CHUNKS)),
        ],
        name="move_weights",
        compiler_params=pltpu.CompilerParams(
            collective_id=0, has_side_effects=True, vmem_limit_bytes=56 << 20
        ),
    )(gain.reshape(rows, 1), w_gate, w_up, w_down)


def mix_kernel(rows_ref, weight_ref, gate_ref, up_ref, down_ref, gate_out, up_out, down_out, term_ref, total):
    j = pl.program_id(0)

    @pl.when(j == 0)
    def _():
        total[...] = jnp.zeros_like(total)

    gate, up, down = gate_ref[...], up_ref[...], down_ref[...]
    gate_out[...], up_out[...], down_out[...] = gate, up, down
    x = rows_ref[...]
    gate_act = jnp.dot(x, gate, preferred_element_type=F32)
    up_act = jnp.dot(x, up, preferred_element_type=F32)
    scale = weight_ref[:, :1].astype(F32)
    hidden = (gate_act / (1.0 + jnp.exp(-gate_act)) * up_act * scale).astype(BF16)
    total[...] += jnp.dot(hidden, down, preferred_element_type=F32)

    @pl.when(j == pl.num_programs(0) - 1)
    def _():
        term_ref[...] = total[...].astype(BF16)


def mix(packed, depth, gate, up, down):
    count = packed.shape[0]
    cols = gate.shape[1]
    wide = down.shape[1]
    tile = next(w for w in (256, 128) if cols % w == 0)
    whole = pl.BlockSpec((count, depth), lambda j: (0, 0))
    column = pl.BlockSpec((depth, tile), lambda j: (0, j))
    row = pl.BlockSpec((tile, wide), lambda j: (j, 0))
    return pl.pallas_call(
        mix_kernel,
        grid=(cols // tile,),
        out_shape=(
            jax.ShapeDtypeStruct(gate.shape, BF16),
            jax.ShapeDtypeStruct(up.shape, BF16),
            jax.ShapeDtypeStruct(down.shape, BF16),
            jax.ShapeDtypeStruct((count, wide), BF16),
        ),
        in_specs=[whole, pl.BlockSpec((count, 128), lambda j: (0, depth // 128)), column, column, row],
        out_specs=(column, column, row, pl.BlockSpec((count, wide), lambda j: (0, 0))),
        scratch_shapes=[pltpu.VMEM((count, wide), F32)],
        name="mix_tokens",
        compiler_params=pltpu.CompilerParams(vmem_limit_bytes=48 << 20),
    )(packed, packed, gate, up, down)


def sum_kernel(n, term_ref, out_ref, near, near_in, far, far_in, last, last_in, s1, r1, s2, r2, s3, r3):
    g, f, t = lax.axis_index("grp"), lax.axis_index("fs"), lax.axis_index("tp")
    mesh_id = pl.DeviceIdType.MESH
    width = out_ref.shape[1]
    count = out_ref.shape[0]
    mate = t + 1 - 2 * lax.rem(t, 2)
    over = lax.rem(t + 2, n)
    mate_over = lax.rem(mate + 2, n)

    barrier = pltpu.get_barrier_semaphore()
    for e in (mate, over):
        pl.semaphore_signal(barrier, inc=1, device_id=(g, f, e), device_id_type=mesh_id)
    for d in range(1, n):
        pl.semaphore_signal(barrier, inc=1, device_id=(g, lax.rem(f + d, n), t), device_id_type=mesh_id)
    pl.semaphore_wait(barrier, n + 1)

    def block(layer, column):
        return term_ref.at[pl.ds(pl.multiple_of(layer * count, count), count), pl.ds(pl.multiple_of(column * width, width), width)]

    def remote(src, dst, ssem, rsem, where):
        return pltpu.make_async_remote_copy(
            src_ref=src, dst_ref=dst, send_sem=ssem, recv_sem=rsem, device_id=where, device_id_type=mesh_id
        )

    layers = [lax.rem(f + d, n) for d in (2, 1, 3, 0)]

    def to_mate(i, h):
        column = mate_over if h == 0 else mate
        return remote(block(layers[i], column), near_in.at[h, i], s1.at[h, i], r1.at[h, i], (g, f, mate))

    def to_over(i):
        return remote(far.at[i], far_in.at[i], s2.at[i], r2.at[i], (g, f, over))

    def to_layer(i):
        return remote(last.at[i], last_in.at[f], s3.at[i], r3.at[f], (g, layers[i], t))

    def from_layer(layer):
        return remote(last.at[0], last_in.at[layer], s3.at[0], r3.at[layer], (g, layer, t))

    for i in range(n):
        for h in range(2):
            to_mate(i, h).start()
    for i in range(n):
        to_mate(i, 0).wait_recv()
        far[i] = (block(layers[i], over)[...].astype(F32) + near_in[0, i].astype(F32)).astype(BF16)
        to_mate(i, 1).wait_recv()
        near[i] = block(layers[i], t)[...].astype(F32) + near_in[1, i].astype(F32)
        to_over(i).start()
    for i in range(n):
        to_over(i).wait_recv()
        near[i] = near[i] + far_in[i].astype(F32)
        if i < n - 1:
            last[i] = near[i].astype(BF16)
            to_layer(i).start()
    total = near[n - 1]
    for d in range(1, n):
        layer = lax.rem(f + d, n)
        from_layer(layer).wait_recv()
        total = total + last_in[layer].astype(F32)
    out_ref[...] = total.astype(BF16)
    for i in range(n):
        for h in range(2):
            to_mate(i, h).wait_send()
        to_over(i).wait_send()
        if i < n - 1:
            to_layer(i).wait_send()


def sum_terms(n, term):
    count, width = term.shape[0] // n, term.shape[1] // n
    dma = pltpu.SemaphoreType.DMA
    vmem = pl.BlockSpec(memory_space=pltpu.VMEM)
    piece = (count, width)
    return pl.pallas_call(
        functools.partial(sum_kernel, n),
        out_shape=jax.ShapeDtypeStruct(piece, BF16),
        in_specs=[vmem],
        out_specs=vmem,
        scratch_shapes=[
            pltpu.VMEM((n, *piece), F32),
            pltpu.VMEM((2, n, *piece), BF16),
            pltpu.VMEM((n, *piece), BF16),
            pltpu.VMEM((n, *piece), BF16),
            pltpu.VMEM((n, *piece), BF16),
            pltpu.VMEM((n, *piece), BF16),
            dma((2, n)), dma((2, n)), dma((n,)), dma((n,)), dma((n,)), dma((n,)),
        ],
        name="sum_terms",
        compiler_params=pltpu.CompilerParams(collective_id=1, has_side_effects=True),
    )(term)


def fits(mesh, tokens, w_gate, w_down):
    groups, n, tp = mesh.shape["grp"], mesh.shape["fs"], mesh.shape["tp"]
    rows, cols = w_gate.shape[1:]
    hidden, width = w_down.shape[1:]
    return (
        groups == 2 and n == 4 and tp == 4 and w_gate.shape[0] == tp
        and cols == hidden and cols % 128 == 0 and width % 128 == 0 and tokens.shape[0] % 16 == 0
        and rows % (groups * CHUNKS * 16) == 0 and hidden % (DOWN_CHUNKS * 16) == 0
        and tokens.shape[0] * n <= 512
    )


def body(mesh, tokens, routes, route_logits, gain, w_gate, w_up, w_down):
    values = tokens.astype(F32)
    mean_square = jnp.mean(values * values, axis=-1, keepdims=True)
    normed = (values * lax.rsqrt(mean_square + 1e-06)).astype(BF16)
    expert_id = lax.axis_index("tp")
    first = jax.nn.sigmoid(route_logits[:, 0] - route_logits[:, 1])
    second = jax.nn.sigmoid(route_logits[:, 1] - route_logits[:, 0])
    weight_col = first * (routes[:, 0] == expert_id).astype(F32)
    weight_col = (weight_col + second * (routes[:, 1] == expert_id).astype(F32)).astype(BF16)
    packed = jnp.concatenate([normed, jnp.broadcast_to(weight_col[:, None], (normed.shape[0], 128))], axis=1)
    packed = lax.all_gather(packed, "fs", axis=0, tiled=True)
    n, depth = mesh.shape["fs"], normed.shape[1]
    if fits(mesh, tokens, w_gate, w_down):
        gate, up, down = move(mesh.shape["grp"], n, gain, w_gate, w_up, w_down)
        gate, up, down, term = mix(packed, depth, gate, up, down)
        return gate[None], up[None], down[None], sum_terms(n, term)
    gate = (w_gate * gain[None, :, None]).astype(BF16)
    up = (w_up * gain[None, :, None]).astype(BF16)
    spread = functools.partial(lax.all_to_all, axis_name="tp", split_axis=0, concat_axis=2, tiled=True)
    gate, up, down = spread(gate), spread(up), spread(w_down.astype(BF16))
    stack = functools.partial(lax.all_to_all, axis_name="fs", split_axis=2, concat_axis=1, tiled=True)
    gate, up = stack(gate), stack(up)
    rows, weight = packed[:, :depth], packed[:, depth : depth + 1]
    gate_act = jnp.dot(rows, gate[0], preferred_element_type=F32)
    up_act = jnp.dot(rows, up[0], preferred_element_type=F32)
    hidden = (jax.nn.silu(gate_act) * up_act * weight.astype(F32)).astype(BF16)
    term = jnp.dot(hidden, down[0], preferred_element_type=F32)
    by_feature = lax.psum_scatter(term, "tp", scatter_dimension=1, tiled=True)
    mixed = lax.psum_scatter(by_feature, "fs", scatter_dimension=0, tiled=True)
    return gate, up, down, mixed.astype(BF16)


def solution(mesh):
    return jax.shard_map(
        functools.partial(body, mesh),
        mesh=mesh,
        in_specs=(
            P(("grp", "fs"), None),
            P(("grp", "fs"), None),
            P(("grp", "fs"), None),
            P("fs"),
            P(None, "fs", "tp"),
            P(None, "fs", "tp"),
            P(None, "fs", "tp"),
        ),
        out_specs=(
            P(("grp", "tp"), None, "fs"),
            P(("grp", "tp"), None, "fs"),
            P(("grp", "tp"), "fs", None),
            P(("grp", "fs"), "tp"),
        ),
        check_vma=False,
    )
```

profile of v0, /device:TPU:0, one launch (start us, length us, event | category | flops | bytes accessed | tf_op | source)
XLA Modules:
  0.0 279.6 jit_solution(4929194741640382689)
XLA Ops:
  7.2 0.0 all-gather.2.cloned.1.call-start
  7.2 1.1 fusion
  8.3 1.1 fusion.1
  9.4 0.8 convert_bitcast_fusion
  10.2 0.1 broadcast_in_dim.19
  10.3 0.7 pad_maximum_fusion
  11.0 0.0 all-gather.2.cloned.1.call-update
  11.0 1.5 copy.11.gain_ref
  12.6 167.6 %move_weights.1 = (bf16[2048,1792]{1,0:T(8,128)(2,1)}, bf16[2048,1792]{1,0:T(8,128)(2,1)}, bf16[1792,2048]{1,0:T(8,128)(2,1)}) custom-call(f32[512,1]{1,0:T(8,128)} %copy.11.gain_ref, f32[4,512,1792]{2,1,0:T(8,128)} %wg_ref.1, f32[4,512,1792]{2,1,0:T(8,128)} %wu_ref.1, f32[4,1792,512]{2,1,0:T(8,128)} %wd_ref.1), custom_call_target="tpu_custom_call" | custom-call | tf_op jit(solution)/shard_map/move_weights/pallas_call | solution.py:277
  180.2 0.0 all-gather.2.cloned.1.call-done.rows_ref.weight_ref
  180.2 0.0 copy-start
  180.2 1.2 copy-done
  181.4 20.5 %mix_tokens.1 = (bf16[2048,1792]{1,0:T(8,128)(2,1)}, bf16[2048,1792]{1,0:T(8,128)(2,1)}, bf16[1792,2048]{1,0:T(8,128)(2,1)}, bf16[256,2048]{1,0:T(8,128)(2,1)S(1)}) custom-call(bf16[256,2176]{1,0:T(8,128)(2,1)S(1)} %copy-done, bf16[256,2176]{1,0:T(8,128)(2,1)S(1)} %copy-done, bf16[2048,1792]{1,0:T(8,128)(2,1)} %get-tuple-element.11.gate_ref, ...), custom_call_target="tpu_custom_call" | custom-call | tf_op jit(solution)/shard_map/mix_tokens/pallas_call | solution.py:341
  201.9 0.0 copy-start.1
  201.9 1.0 copy-done.1
  202.9 68.4 %sum_terms.1 = bf16[64,512]{1,0:T(8,128)(2,1)} custom-call(bf16[256,2048]{1,0:T(8,128)(2,1)} %copy-done.1), custom_call_target="tpu_custom_call" | custom-call | tf_op jit(solution)/shard_map/sum_terms/pallas_call | solution.py:431
  271.3 1.5 copy.13
  (1 shorter events, 0.0 us)
Async XLA Ops:
  7.2 173.0 %all-gather.2.cloned.1.call-start = ((), (), s32[]{:S(2)}) async-start(), calls=%async_computation | async-start | bytes 1392640 | tf_op jit(solution)/shard_map/all_gather | solution.py:472
  180.2 1.2 copy-start
  201.9 1.0 copy-start.1
Sparse Core Ops, SparseCore 0:
  11.1 87.5 all-gather.1
where the time goes:
time: 281 us; the launch traced here: 280 us
  Pallas kernels  256 us (91%)
  between operations  14.1 us (5%)
  local copies, waits for them, and re-layouts  5.29 us (2%)
  other arithmetic  3.7 us (1%)
    pallas_call x1, Pallas kernels, move(): pl.pallas_call(functools.partial(move_kernel, groups, n), out_shape=(jax....  168 us
    pallas_call x1, Pallas kernels, sum_terms(): pl.pallas_call(functools.partial(sum_kernel, n), out_shape=jax.ShapeDtype...  68.4 us
    pallas_call x1, Pallas kernels, mix(): pl.pallas_call(mix_kernel, grid=(cols // tile,), out_shape=(jax.ShapeDtyp...  20.5 us
  transfers between devices with their start and end apart: 1, of which 0 were waited for; matrix products, arithmetic and copies ran while one was open for 1% of the time, Pallas kernels for 60%

commit v1 on v0

v1 whole, which is shorter than its diff:
```python
import functools

import jax
import jax.numpy as jnp
from jax import lax
from jax.experimental import pallas as pl
from jax.experimental.pallas import tpu as pltpu
from jax.sharding import PartitionSpec as P

BF16 = jnp.bfloat16
F32 = jnp.float32
CHUNKS = 4
DOWN_CHUNKS = 4
LOADS = 3
DOWN_LOADS = 2
STEPS = 18
OUTER_LEAD = 2
OUTER_OWN = (0, 0, 1, 1, 2, 2, 3, 4, 6)
OUTER_RELAY = (1, 1, 2, 2, 3, 3, 4, 5, 8)
NEAR_LAG = 1
IN_RATE, IN_LAG = 0.6, 1.0
OUT_RATE, OUT_LAG = 0.5, 0.8
LANES = 128


def move_kernel(
    groups, n, tokens_ref, routes_ref, logits_ref, gain_ref, wg_ref, wu_ref, wd_ref, x_ref, gu_ref, od_ref,
    wide, wide_d, stage, extra, relay, stage_d, tok, pack, route_v, logit_v, gain_v, gain_col,
    load_sem, load_d_sem, small_sem, s1s, s1r, xs, xr, zs, zr, ys, yr, ds, dr, ts, tr, os, ov, ms, mr, own_sem,
):
    g, f, t = lax.axis_index("grp"), lax.axis_index("fs"), lax.axis_index("tp")
    rows = wg_ref.shape[1]
    half = rows // groups
    ch = half // CHUNKS
    hidden, width = wd_ref.shape[1:]
    dh = hidden // DOWN_CHUNKS
    items = 2 * CHUNKS
    count, depth = tokens_ref.shape
    part = count // n
    weights = (wg_ref, wu_ref)

    core = lax.rem(t, 2)
    mate = t + 1 - 2 * core
    peers = (t, mate, lax.rem(t + 2, n), lax.rem(mate + 2, n))
    home = f == t
    order = (2, 3, 0, 1)
    near = f + 1 - 2 * lax.rem(f, 2)
    low = f < n // 2
    far = (jnp.where(low, 2, 1), jnp.where(low, 3, 0))

    def remote(src, dst, ssem, rsem, where):
        return pltpu.make_async_remote_copy(
            src_ref=src, dst_ref=dst, send_sem=ssem, recv_sem=rsem,
            device_id=where, device_id_type=pl.DeviceIdType.MESH,
        )

    def own_row(c):
        return pl.multiple_of(g * half + c * ch, ch)

    def other_row(c):
        return pl.multiple_of((1 - g) * half + c * ch, ch)

    def load(i, k, row):
        slot = i % LOADS
        src = weights[i // CHUNKS].at[peers[k], pl.ds(row(i % CHUNKS), ch), :]
        return pltpu.make_async_copy(src, wide.at[slot, k], load_sem.at[slot, k])

    for i in range(LOADS):
        for k in order:
            load(i, k, own_row).start()
    small = (
        pltpu.make_async_copy(gain_ref, gain_v, small_sem.at[0]),
        pltpu.make_async_copy(tokens_ref, tok, small_sem.at[1]),
        pltpu.make_async_copy(routes_ref, route_v, small_sem.at[2]),
        pltpu.make_async_copy(logits_ref, logit_v, small_sem.at[3]),
    )
    for copy in small:
        copy.start()

    barrier = pltpu.get_barrier_semaphore()

    def greet(where):
        pl.semaphore_signal(barrier, inc=1, device_id=where, device_id_type=pl.DeviceIdType.MESH)

    for k in (1, 2, 3):
        greet((g, f, peers[k]))
    for d in range(1, n):
        for k in (0, 1):
            greet((g, lax.rem(f + d, n), peers[k]))
    greet((1 - g, f, t))

    small[0].wait()
    for b in range(rows // LANES):
        line = gain_v[0:1, b * LANES : (b + 1) * LANES]
        eye = lax.broadcasted_iota(jnp.int32, (LANES, LANES), 0) == lax.broadcasted_iota(jnp.int32, (LANES, LANES), 1)
        column = jnp.sum(jnp.where(eye, jnp.broadcast_to(line, (LANES, LANES)), 0.0), axis=1, keepdims=True)
        gain_col[b * LANES : (b + 1) * LANES, :] = jnp.broadcast_to(column, (LANES, LANES))
    pl.semaphore_wait(barrier, 2 * n + 2)

    def at_rows(i, source, row):
        start = i // CHUNKS * (rows * n) + source * rows + row
        return gu_ref.at[pl.ds(pl.multiple_of(start, ch), ch), :]

    def own_piece(i, source):
        return at_rows(i, source, own_row(i % CHUNKS))

    def other_piece(i, source):
        return at_rows(i, source, other_row(i % CHUNKS))

    def first(k, i):
        return remote(stage.at[k, i], relay.at[k - 2, i], s1s.at[k, i], s1r.at[k, i], (g, f, peers[k]))

    def first_home(k, i):
        return remote(stage.at[k, i], own_piece(i, f), s1s.at[k, i], s1r.at[k, i], (g, f, peers[k]))

    def own_home(i):
        return pltpu.make_async_copy(stage.at[0, i], own_piece(i, f), s1s.at[0, i])

    def direct(k, i):
        return remote(stage.at[k, i], own_piece(i, f), zs.at[k, i], zr.at[f, i], (g, t, peers[k]))

    def layer(k, i):
        return remote(relay.at[k - 2, i], own_piece(i, f), zs.at[k, i], zr.at[f, i], (g, peers[k], t))

    def layer_in(source, i):
        piece = own_piece(i, source)
        return remote(piece, piece, zs.at[0, i], zr.at[source, i], (1 - g, f, t))

    def across(source, i):
        piece = own_piece(i, source)
        return remote(piece, piece, ys.at[source, i], yr.at[source, i], (1 - g, f, t))

    def extra_home(i):
        return pltpu.make_async_copy(extra.at[0, i], other_piece(i, f), xs.at[0, i])

    def extra_mate(i):
        return remote(extra.at[1, i], other_piece(i, f), xs.at[1, i], xr.at[i], (g, f, mate))

    def down(k, c):
        src = stage_d.at[k, c]
        dst = od_ref.at[pl.ds(c * dh, dh), pl.ds(pl.multiple_of(t * width, LANES), width)]
        if k == 0:
            return pltpu.make_async_copy(src, dst, ds.at[0, c])
        return remote(src, dst, ds.at[k, c], dr.at[k, c], (g, f, peers[k]))

    def load_d(k, c):
        slot = c % DOWN_LOADS
        return pltpu.make_async_copy(wd_ref.at[peers[k], pl.ds(c * dh, dh), :], wide_d.at[slot, k], load_d_sem.at[slot, k])

    def fold(slot, k, row, dst):
        scale = gain_col[pl.ds(row, ch), 0:1]
        dst[...] = (wide[slot, k] * scale).astype(BF16)

    def piece(source, q):
        return x_ref.at[pl.ds(pl.multiple_of(source * count + q * part, part), part), :]

    def token_out(d):
        src = pack.at[pl.ds(pl.multiple_of(t * part, part), part), :]
        return remote(src, piece(f, t), ts.at[d], tr.at[f], (g, lax.rem(f + d, n), t))

    def token_in(source):
        return remote(piece(source, t), piece(source, t), ts.at[0], tr.at[source], (g, f, t))

    def token_over(source):
        here = piece(source, t)
        return remote(here, here, os.at[source], ov.at[source], (g, f, peers[2]))

    def token_from_over(source):
        here = piece(source, peers[2])
        return remote(here, here, os.at[source], ov.at[source], (g, f, peers[2]))

    def token_mate(source, j):
        here = piece(source, (t, peers[2])[j])
        return remote(here, here, ms.at[j, source], mr.at[j, source], (g, f, mate))

    def token_from_mate(source, j):
        here = piece(source, (mate, peers[3])[j])
        return remote(here, here, ms.at[j, source], mr.at[j, source], (g, f, mate))

    def token_own():
        return pltpu.make_async_copy(pack, x_ref.at[pl.ds(pl.multiple_of(f * count, count), count), :], own_sem.at[0])

    def send_tokens():
        for copy in small[1:]:
            copy.wait()
        values = tok[...].astype(F32)
        mean_square = jnp.mean(values * values, axis=-1, keepdims=True)
        pack[:, :depth] = (values * lax.rsqrt(mean_square + 1e-06)).astype(BF16)
        diff = logit_v[0:1, :] - logit_v[1:2, :]
        first_w = 1.0 / (1.0 + jnp.exp(-diff))
        second_w = 1.0 / (1.0 + jnp.exp(diff))
        eye = lax.broadcasted_iota(jnp.int32, (count, count), 0) == lax.broadcasted_iota(jnp.int32, (count, count), 1)
        lane = lax.broadcasted_iota(jnp.int32, (count, LANES), 1)
        table = jnp.zeros((count, LANES), F32)
        for e in range(n):
            line = first_w * (route_v[0:1, :] == e).astype(F32) + second_w * (route_v[1:2, :] == e).astype(F32)
            column = jnp.sum(jnp.where(eye, jnp.broadcast_to(line, (count, count)), 0.0), axis=1, keepdims=True)
            table = jnp.where(lane == e, jnp.broadcast_to(column, (count, LANES)), table)
        pack[:, depth:] = table.astype(BF16)
        token_own().start()
        for d in range(1, n):
            token_out(d).start()

    def share_tokens():
        for d in range(1, n):
            source = lax.rem(f + d, n)
            token_in(source).wait_recv()
            token_over(source).start()
            token_mate(source, 0).start()

    def pair_tokens():
        for d in range(1, n):
            source = lax.rem(f + d, n)
            token_from_over(source).wait_recv()
            token_mate(source, 1).start()

    def produce(i):
        for k in order:
            load(i, k, own_row).wait()
            fold(i % LOADS, k, own_row(i % CHUNKS), stage.at[k, i])
            if i + LOADS < items:
                load(i + LOADS, k, own_row).start()

            @pl.when(home)
            def _():
                if k == 0:
                    own_home(i).start()
                else:
                    first_home(k, i).start()

            if k >= 2:
                @pl.when(jnp.logical_not(home))
                def _():
                    first(k, i).start()

    def own(i, where):
        @pl.when(where)
        def _():
            direct(0, i).start()
            direct(1, i).start()

    def relay_home(i):
        for k in (2, 3):
            @pl.when(peers[k] == f)
            def _():
                first_home(k, i).wait_recv()
                across(f, i).start()

    def relay_near(i):
        for k in (2, 3):
            @pl.when(peers[k] == near)
            def _():
                first(k, i).wait_recv()
                layer(k, i).start()

    def relay_far(i, where):
        for k in (2, 3):
            @pl.when(where & (peers[k] != f) & (peers[k] != near))
            def _():
                first(k, i).wait_recv()
                layer(k, i).start()

    def turn(source, i):
        layer_in(source, i).wait_recv()
        across(source, i).start()

    def down_step(c):
        for k in order:
            load_d(k, c).wait()
            stage_d[k, c] = wide_d[c % DOWN_LOADS, k].astype(BF16)
            if c + DOWN_LOADS < DOWN_CHUNKS:
                load_d(k, c + DOWN_LOADS).start()
            down(k, c).start()

    def home_step(i):
        for k in (0, 1):
            load(i, k, other_row).wait()
            fold(i % LOADS, k, other_row(i % CHUNKS), extra.at[k, i])
            if i + LOADS < items:
                load(i + LOADS, k, other_row).start()
            (extra_home if k == 0 else extra_mate)(i).start()

    outer = (f == 0) | (f == n - 1)
    inner = jnp.logical_not(outer)
    own_far = (t != near) & jnp.logical_not(home)
    send_tokens()
    for i in range(items):
        produce(i)
        own(i, t == near)
        own(i, own_far & inner)
        if i < OUTER_LEAD:
            own(i, own_far & outer)
        if i == 1:
            for c in range(DOWN_LOADS):
                for k in order:
                    load_d(k, c).start()
    sent = {"own": OUTER_LEAD, "relay": 0, "near": 0, "in": 0, "out": 0}

    def up_to(name, limit, act):
        while sent[name] < min(limit, items):
            act(sent[name])
            sent[name] += 1

    for s in range(STEPS):
        if s < items:
            relay_home(s)
            relay_near(s)
            relay_far(s, inner)
        up_to("own", OUTER_LEAD + OUTER_OWN[min(s, len(OUTER_OWN) - 1)], lambda i: own(i, own_far & outer))
        up_to("relay", OUTER_RELAY[min(s, len(OUTER_RELAY) - 1)], lambda i: relay_far(i, outer))
        if s == 0:
            share_tokens()
        if 1 <= s <= DOWN_CHUNKS:
            down_step(s - 1)
        if s == items + 1:
            pair_tokens()
        up_to("near", s + 1 - NEAR_LAG, lambda i: turn(near, i))
        up_to("in", int((s + 1) * IN_RATE - IN_LAG), lambda i: turn(far[0], i))
        up_to("out", int((s + 1) * OUT_RATE - OUT_LAG), lambda i: turn(far[1], i))
        if s == items:
            @pl.when(home)
            def _():
                for j in range(LOADS):
                    for k in (0, 1):
                        load(j, k, other_row).start()
                for j in range(items):
                    home_step(j)
    assert min(sent.values()) == items

    def finish(i, _):
        @pl.when(home)
        def _():
            own_home(i).wait()
            extra_home(i).wait()
            extra_mate(i).wait_send()
            first_home(1, i).wait_send()

        @pl.when(jnp.logical_not(home))
        def _():
            direct(0, i).wait_send()
            direct(1, i).wait_send()

        @pl.when(f == mate)
        def _():
            first_home(1, i).wait_recv()
            extra_mate(i).wait_recv()

        for k in (2, 3):
            first(k, i).wait_send()

            @pl.when(peers[k] != f)
            def _():
                layer(k, i).wait_send()

            @pl.when(peers[k] == f)
            def _():
                across(f, i).wait()

        for source in (near, *far):
            across(source, i).wait()
        return 0

    lax.fori_loop(0, items, finish, 0)

    def finish_d(c, _):
        for k in range(n):
            down(k, c).wait()
        return 0

    lax.fori_loop(0, DOWN_CHUNKS, finish_d, 0)
    token_own().wait()
    for d in range(1, n):
        source = lax.rem(f + d, n)
        token_out(d).wait_send()
        token_over(source).wait_send()
        for j in range(2):
            token_mate(source, j).wait_send()
            token_from_mate(source, j).wait_recv()


def move(groups, n, tokens, routes, route_logits, gain, w_gate, w_up, w_down):
    experts, rows, cols = w_gate.shape
    hidden, width = w_down.shape[1:]
    count, depth = tokens.shape
    ch = rows // groups // CHUNKS
    dh = hidden // DOWN_CHUNKS
    items = 2 * CHUNKS
    dma = pltpu.SemaphoreType.DMA
    hbm = pl.BlockSpec(memory_space=pl.ANY)
    return pl.pallas_call(
        functools.partial(move_kernel, groups, n),
        out_shape=(
            jax.ShapeDtypeStruct((count * n, depth + LANES), BF16),
            jax.ShapeDtypeStruct((2 * rows * n, cols), BF16),
            jax.ShapeDtypeStruct((hidden, width * n), BF16),
        ),
        in_specs=[hbm] * 7,
        out_specs=(hbm, hbm, hbm),
        scratch_shapes=[
            pltpu.VMEM((LOADS, n, ch, cols), F32),
            pltpu.VMEM((DOWN_LOADS, n, dh, width), F32),
            pltpu.VMEM((n, items, ch, cols), BF16),
            pltpu.VMEM((2, items, ch, cols), BF16),
            pltpu.VMEM((2, items, ch, cols), BF16),
            pltpu.VMEM((n, DOWN_CHUNKS, dh, width), BF16),
            pltpu.VMEM((count, depth), BF16),
            pltpu.VMEM((count, depth + LANES), BF16),
            pltpu.VMEM((2, count), jnp.int32),
            pltpu.VMEM((2, count), F32),
            pltpu.VMEM((1, rows), F32),
            pltpu.VMEM((rows, LANES), F32),
            dma((LOADS, n)),
            dma((DOWN_LOADS, n)),
            dma((4,)),
            dma((n, items)),
            dma((n, items)),
            dma((2, items)),
            dma((items,)),
            dma((n, items)),
            dma((n, items)),
            dma((n, items)),
            dma((n, items)),
            dma((n, DOWN_CHUNKS)),
            dma((n, DOWN_CHUNKS)),
            dma((n,)),
            dma((n,)),
            dma((n,)),
            dma((n,)),
            dma((2, n)),
            dma((2, n)),
            dma((1,)),
        ],
        name="move_weights",
        compiler_params=pltpu.CompilerParams(
            collective_id=0, has_side_effects=True, vmem_limit_bytes=56 << 20
        ),
    )(tokens, routes.T, route_logits.T, gain.reshape(1, rows), w_gate, w_up, w_down)


def mix_kernel(rows_ref, weight_ref, gate_ref, up_ref, down_ref, gate_out, up_out, down_out, term_ref, total):
    j = pl.program_id(0)

    @pl.when(j == 0)
    def _():
        total[...] = jnp.zeros_like(total)

    gate, up, down = gate_ref[...], up_ref[...], down_ref[...]
    gate_out[...], up_out[...], down_out[...] = gate, up, down
    x = rows_ref[...]
    gate_act = jnp.dot(x, gate, preferred_element_type=F32)
    up_act = jnp.dot(x, up, preferred_element_type=F32)
    lane = lax.broadcasted_iota(jnp.int32, weight_ref.shape, 1)
    table = jnp.where(lane == lax.axis_index("tp"), weight_ref[...].astype(F32), 0.0)
    scale = jnp.sum(table, axis=1, keepdims=True)
    hidden = (gate_act / (1.0 + jnp.exp(-gate_act)) * up_act * scale).astype(BF16)
    total[...] += jnp.dot(hidden, down, preferred_element_type=F32)

    @pl.when(j == pl.num_programs(0) - 1)
    def _():
        term_ref[...] = total[...].astype(BF16)


def mix(packed, both, down):
    count, depth = packed.shape[0], packed.shape[1] - LANES
    cols = both.shape[1]
    wide = down.shape[1]
    tile = next(w for w in (256, 128) if cols % w == 0)
    whole = pl.BlockSpec((count, depth), lambda j: (0, 0))
    column = pl.BlockSpec((depth, tile), lambda j: (0, j))
    second = pl.BlockSpec((depth, tile), lambda j: (1, j))
    row = pl.BlockSpec((tile, wide), lambda j: (j, 0))
    return pl.pallas_call(
        mix_kernel,
        grid=(cols // tile,),
        out_shape=(
            jax.ShapeDtypeStruct((depth, cols), BF16),
            jax.ShapeDtypeStruct((depth, cols), BF16),
            jax.ShapeDtypeStruct(down.shape, BF16),
            jax.ShapeDtypeStruct((count, wide), BF16),
        ),
        in_specs=[whole, pl.BlockSpec((count, LANES), lambda j: (0, depth // LANES)), column, second, row],
        out_specs=(column, column, row, pl.BlockSpec((count, wide), lambda j: (0, 0))),
        scratch_shapes=[pltpu.VMEM((count, wide), F32)],
        name="mix_tokens",
        compiler_params=pltpu.CompilerParams(vmem_limit_bytes=48 << 20),
    )(packed, packed, both, both, down)


def sum_kernel(n, term_ref, out_ref, near, near_in, far, far_in, last, last_in, s1, r1, s2, r2, s3, r3):
    g, f, t = lax.axis_index("grp"), lax.axis_index("fs"), lax.axis_index("tp")
    mesh_id = pl.DeviceIdType.MESH
    width = out_ref.shape[1]
    count = out_ref.shape[0]
    mate = t + 1 - 2 * lax.rem(t, 2)
    over = lax.rem(t + 2, n)
    mate_over = lax.rem(mate + 2, n)

    barrier = pltpu.get_barrier_semaphore()
    for e in (mate, over):
        pl.semaphore_signal(barrier, inc=1, device_id=(g, f, e), device_id_type=mesh_id)
    for d in range(1, n):
        pl.semaphore_signal(barrier, inc=1, device_id=(g, lax.rem(f + d, n), t), device_id_type=mesh_id)
    pl.semaphore_wait(barrier, n + 1)

    def block(layer, column):
        return term_ref.at[pl.ds(pl.multiple_of(layer * count, count), count), pl.ds(pl.multiple_of(column * width, width), width)]

    def remote(src, dst, ssem, rsem, where):
        return pltpu.make_async_remote_copy(
            src_ref=src, dst_ref=dst, send_sem=ssem, recv_sem=rsem, device_id=where, device_id_type=mesh_id
        )

    layers = [lax.rem(f + d, n) for d in (2, 1, 3, 0)]

    def to_mate(i, h):
        column = mate_over if h == 0 else mate
        return remote(block(layers[i], column), near_in.at[h, i], s1.at[h, i], r1.at[h, i], (g, f, mate))

    def to_over(i):
        return remote(far.at[i], far_in.at[i], s2.at[i], r2.at[i], (g, f, over))

    def to_layer(i):
        return remote(last.at[i], last_in.at[f], s3.at[i], r3.at[f], (g, layers[i], t))

    def from_layer(layer):
        return remote(last.at[0], last_in.at[layer], s3.at[0], r3.at[layer], (g, layer, t))

    for i in range(n):
        for h in range(2):
            to_mate(i, h).start()
    for i in range(n):
        to_mate(i, 0).wait_recv()
        far[i] = (block(layers[i], over)[...].astype(F32) + near_in[0, i].astype(F32)).astype(BF16)
        to_mate(i, 1).wait_recv()
        near[i] = block(layers[i], t)[...].astype(F32) + near_in[1, i].astype(F32)
        to_over(i).start()
    for i in range(n):
        to_over(i).wait_recv()
        near[i] = near[i] + far_in[i].astype(F32)
        if i < n - 1:
            last[i] = near[i].astype(BF16)
            to_layer(i).start()
    total = near[n - 1]
    for d in range(1, n):
        layer = lax.rem(f + d, n)
        from_layer(layer).wait_recv()
        total = total + last_in[layer].astype(F32)
    out_ref[...] = total.astype(BF16)
    for i in range(n):
        for h in range(2):
            to_mate(i, h).wait_send()
        to_over(i).wait_send()
        if i < n - 1:
            to_layer(i).wait_send()


def sum_terms(n, term):
    count, width = term.shape[0] // n, term.shape[1] // n
    dma = pltpu.SemaphoreType.DMA
    vmem = pl.BlockSpec(memory_space=pltpu.VMEM)
    piece = (count, width)
    return pl.pallas_call(
        functools.partial(sum_kernel, n),
        out_shape=jax.ShapeDtypeStruct(piece, BF16),
        in_specs=[vmem],
        out_specs=vmem,
        scratch_shapes=[
            pltpu.VMEM((n, *piece), F32),
            pltpu.VMEM((2, n, *piece), BF16),
            pltpu.VMEM((n, *piece), BF16),
            pltpu.VMEM((n, *piece), BF16),
            pltpu.VMEM((n, *piece), BF16),
            pltpu.VMEM((n, *piece), BF16),
            dma((2, n)), dma((2, n)), dma((n,)), dma((n,)), dma((n,)), dma((n,)),
        ],
        name="sum_terms",
        compiler_params=pltpu.CompilerParams(collective_id=1, has_side_effects=True),
    )(term)


def fits(mesh, tokens, w_gate, w_down):
    groups, n, tp = mesh.shape["grp"], mesh.shape["fs"], mesh.shape["tp"]
    rows, cols = w_gate.shape[1:]
    hidden, width = w_down.shape[1:]
    return (
        groups == 2 and n == 4 and tp == 4 and w_gate.shape[0] == tp
        and cols == hidden and cols % 128 == 0 and width % 128 == 0 and tokens.shape[0] % (16 * n) == 0
        and rows % (groups * CHUNKS * 16) == 0 and hidden % (DOWN_CHUNKS * 16) == 0
        and tokens.shape[0] * n <= 512 and rows % LANES == 0 and rows * n == tokens.shape[1]
    )


def body(mesh, tokens, routes, route_logits, gain, w_gate, w_up, w_down):
    n, depth = mesh.shape["fs"], tokens.shape[1]
    if fits(mesh, tokens, w_gate, w_down):
        packed, both, down = move(mesh.shape["grp"], n, tokens, routes, route_logits, gain, w_gate, w_up, w_down)
        gate, up, down, term = mix(packed, both, down)
        return gate[None], up[None], down[None], sum_terms(n, term)
    values = tokens.astype(F32)
    mean_square = jnp.mean(values * values, axis=-1, keepdims=True)
    normed = (values * lax.rsqrt(mean_square + 1e-06)).astype(BF16)
    expert_id = lax.axis_index("tp")
    first = jax.nn.sigmoid(route_logits[:, 0] - route_logits[:, 1])
    second = jax.nn.sigmoid(route_logits[:, 1] - route_logits[:, 0])
    weight_col = first * (routes[:, 0] == expert_id).astype(F32)
    weight_col = (weight_col + second * (routes[:, 1] == expert_id).astype(F32)).astype(BF16)
    packed = jnp.concatenate([normed, jnp.broadcast_to(weight_col[:, None], (normed.shape[0], 128))], axis=1)
    packed = lax.all_gather(packed, "fs", axis=0, tiled=True)
    gate = (w_gate * gain[None, :, None]).astype(BF16)
    up = (w_up * gain[None, :, None]).astype(BF16)
    spread = functools.partial(lax.all_to_all, axis_name="tp", split_axis=0, concat_axis=2, tiled=True)
    gate, up, down = spread(gate), spread(up), spread(w_down.astype(BF16))
    stack = functools.partial(lax.all_to_all, axis_name="fs", split_axis=2, concat_axis=1, tiled=True)
    gate, up = stack(gate), stack(up)
    rows, weight = packed[:, :depth], packed[:, depth : depth + 1]
    gate_act = jnp.dot(rows, gate[0], preferred_element_type=F32)
    up_act = jnp.dot(rows, up[0], preferred_element_type=F32)
    hidden = (jax.nn.silu(gate_act) * up_act * weight.astype(F32)).astype(BF16)
    term = jnp.dot(hidden, down[0], preferred_element_type=F32)
    by_feature = lax.psum_scatter(term, "tp", scatter_dimension=1, tiled=True)
    mixed = lax.psum_scatter(by_feature, "fs", scatter_dimension=0, tiled=True)
    return gate, up, down, mixed.astype(BF16)


def solution(mesh):
    return jax.shard_map(
        functools.partial(body, mesh),
        mesh=mesh,
        in_specs=(
            P(("grp", "fs"), None),
            P(("grp", "fs"), None),
            P(("grp", "fs"), None),
            P("fs"),
            P(None, "fs", "tp"),
            P(None, "fs", "tp"),
            P(None, "fs", "tp"),
        ),
        out_specs=(
            P(("grp", "tp"), None, "fs"),
            P(("grp", "tp"), None, "fs"),
            P(("grp", "tp"), "fs", None),
            P(("grp", "fs"), "tp"),
        ),
        check_vma=False,
    )
```

time: 281 us -> 229 us (0.81)
  Pallas kernels: 256 us -> 225 us
  between operations: 14.1 us -> 0.66 us
  other arithmetic: 3.7 us -> 0 us
    pallas_call x1, Pallas kernels: 68.4 us -> 19.6 us  [sum_terms(): pl.pallas_call(functools.partial(sum_kernel, n), out_shape=jax.ShapeDtype...]
    pallas_call x1, Pallas kernels: 168 us -> 184 us  [move(): pl.pallas_call(functools.partial(move_kernel, groups, n), out_shape=(jax....]
  transfers between devices with their start and end apart: 1 -> 0, of which waited for: 0 -> 0; matrix products, arithmetic and copies ran while one was open for 1% -> 0% of each run, Pallas kernels for 60% -> 0%
where the time goes in v1:
time: 229 us
  Pallas kernels  225 us (98%)
  local copies, waits for them, and re-layouts  3.68 us (2%)
    pallas_call x1, Pallas kernels, move(): pl.pallas_call(functools.partial(move_kernel, groups, n), out_shape=(jax....  184 us
    pallas_call x1, Pallas kernels, mix(): pl.pallas_call(mix_kernel, grid=(cols // tile,), out_shape=(jax.ShapeDtyp...  20.6 us
    pallas_call x1, Pallas kernels, sum_terms(): pl.pallas_call(functools.partial(sum_kernel, n), out_shape=jax.ShapeDtype...  19.6 us

profile of v1, /device:TPU:0, one launch (start us, length us, event | category | flops | bytes accessed | tf_op | source)
XLA Modules:
  0.0 229.0 jit_solution(5991663308286213003)
XLA Ops:
  0.6 184.4 %move_weights.1 = (bf16[256,2176]{1,0:T(8,128)(2,1)}, bf16[4096,1792]{1,0:T(8,128)(2,1)}, bf16[1792,2048]{1,0:T(8,128)(2,1)}) custom-call(bf16[64,2048]{1,0:T(8,128)(2,1)} %tokens_ref.1, s32[2,64]{1,0:T(2,128)} %bitcast.7, f32[2,64]{1,0:T(2,128)} %bitcast.8, f32[1,512]{1,0:T(1,128)} %bitcast.6, f32[4,512,1792]{2,1,0:T(8,128)} %wg_ref.1, ...), custom_call_target="tpu_custom_call" | custom-call | tf_op jit(solution)/shard_map/move_weights/pallas_call | solution.py:390
  185.0 0.0 copy-start
  185.1 1.2 copy-done
  186.3 20.6 %mix_tokens.1 = (bf16[2048,1792]{1,0:T(8,128)(2,1)}, bf16[2048,1792]{1,0:T(8,128)(2,1)}, bf16[1792,2048]{1,0:T(8,128)(2,1)}, bf16[256,2048]{1,0:T(8,128)(2,1)S(1)}) custom-call(bf16[256,2176]{1,0:T(8,128)(2,1)S(1)} %copy-done, bf16[256,2176]{1,0:T(8,128)(2,1)S(1)} %copy-done, bf16[4096,1792]{1,0:T(8,128)(2,1)} %get-tuple-element.12.gate_ref.up_ref, ...), custom_call_target="tpu_custom_call" | custom-call | tf_op jit(solution)/shard_map/mix_tokens/pallas_call | solution.py:472
  206.9 0.0 copy-start.1
  206.9 1.0 copy-done.1
  207.9 19.6 %sum_terms.1 = bf16[64,512]{1,0:T(8,128)(2,1)} custom-call(bf16[256,2048]{1,0:T(8,128)(2,1)} %copy-done.1), custom_call_target="tpu_custom_call" | custom-call | tf_op jit(solution)/shard_map/sum_terms/pallas_call | solution.py:562
  227.5 1.5 copy.12
Async XLA Ops:
  185.0 1.2 copy-start
  206.9 1.0 copy-start.1

commit v2 on v1

--- a/solution.py
+++ b/solution.py
@@ -24,7 +24,7 @@
 
 
 def move_kernel(
-    groups, n, tokens_ref, routes_ref, logits_ref, gain_ref, wg_ref, wu_ref, wd_ref, x_ref, gu_ref, od_ref,
+    groups, n, tokens_ref, routes_ref, logits_ref, gain_ref, wg_ref, wu_ref, wd_ref, x_ref, og_ref, ou_ref, od_ref,
     wide, wide_d, stage, extra, relay, stage_d, tok, pack, route_v, logit_v, gain_v, gain_col,
     load_sem, load_d_sem, small_sem, s1s, s1r, xs, xr, zs, zr, ys, yr, ds, dr, ts, tr, os, ov, ms, mr, own_sem,
 ):
@@ -98,8 +98,7 @@
     pl.semaphore_wait(barrier, 2 * n + 2)
 
     def at_rows(i, source, row):
-        start = i // CHUNKS * (rows * n) + source * rows + row
-        return gu_ref.at[pl.ds(pl.multiple_of(start, ch), ch), :]
+        return (og_ref, ou_ref)[i // CHUNKS].at[pl.ds(pl.multiple_of(source * rows + row, ch), ch), :]
 
     def own_piece(i, source):
         return at_rows(i, source, own_row(i % CHUNKS))
@@ -327,7 +326,7 @@
                     home_step(j)
     assert min(sent.values()) == items
 
-    def finish(i, _):
+    def finish(i):
         @pl.when(home)
         def _():
             own_home(i).wait()
@@ -358,9 +357,9 @@
 
         for source in (near, *far):
             across(source, i).wait()
-        return 0
-
-    lax.fori_loop(0, items, finish, 0)
+
+    for i in range(items):
+        finish(i)
 
     def finish_d(c, _):
         for k in range(n):
@@ -390,12 +389,13 @@
     return pl.pallas_call(
         functools.partial(move_kernel, groups, n),
         out_shape=(
-            jax.ShapeDtypeStruct((count * n, depth + LANES), BF16),
-            jax.ShapeDtypeStruct((2 * rows * n, cols), BF16),
-            jax.ShapeDtypeStruct((hidden, width * n), BF16),
+            pltpu.VMEM((count * n, depth + LANES), BF16),
+            pltpu.VMEM((rows * n, cols), BF16),
+            pltpu.VMEM((rows * n, cols), BF16),
+            pltpu.VMEM((hidden, width * n), BF16),
         ),
         in_specs=[hbm] * 7,
-        out_specs=(hbm, hbm, hbm),
+        out_specs=(pl.BlockSpec(memory_space=pltpu.VMEM),) * 4,
         scratch_shapes=[
             pltpu.VMEM((LOADS, n, ch, cols), F32),
             pltpu.VMEM((DOWN_LOADS, n, dh, width), F32),
@@ -432,58 +432,60 @@
         ],
         name="move_weights",
         compiler_params=pltpu.CompilerParams(
-            collective_id=0, has_side_effects=True, vmem_limit_bytes=56 << 20
+            collective_id=0, has_side_effects=True, vmem_limit_bytes=40 << 20
         ),
     )(tokens, routes.T, route_logits.T, gain.reshape(1, rows), w_gate, w_up, w_down)
 
 
-def mix_kernel(rows_ref, weight_ref, gate_ref, up_ref, down_ref, gate_out, up_out, down_out, term_ref, total):
-    j = pl.program_id(0)
-
-    @pl.when(j == 0)
-    def _():
-        total[...] = jnp.zeros_like(total)
-
-    gate, up, down = gate_ref[...], up_ref[...], down_ref[...]
-    gate_out[...], up_out[...], down_out[...] = gate, up, down
-    x = rows_ref[...]
-    gate_act = jnp.dot(x, gate, preferred_element_type=F32)
-    up_act = jnp.dot(x, up, preferred_element_type=F32)
-    lane = lax.broadcasted_iota(jnp.int32, weight_ref.shape, 1)
-    table = jnp.where(lane == lax.axis_index("tp"), weight_ref[...].astype(F32), 0.0)
+def mix_kernel(tile, x_ref, gate_ref, up_ref, down_ref, gate_out, up_out, down_out, term_ref, total, out_sem):
+    copies = [
+        pltpu.make_async_copy(src, dst, out_sem.at[i])
+        for i, (src, dst) in enumerate(((gate_ref, gate_out), (up_ref, up_out), (down_ref, down_out)))
+    ]
+    for copy in copies:
+        copy.start()
+    depth = gate_ref.shape[0]
+    lane = lax.broadcasted_iota(jnp.int32, (x_ref.shape[0], LANES), 1)
+    table = jnp.where(lane == lax.axis_index("tp"), x_ref[:, depth:].astype(F32), 0.0)
     scale = jnp.sum(table, axis=1, keepdims=True)
-    hidden = (gate_act / (1.0 + jnp.exp(-gate_act)) * up_act * scale).astype(BF16)
-    total[...] += jnp.dot(hidden, down, preferred_element_type=F32)
-
-    @pl.when(j == pl.num_programs(0) - 1)
-    def _():
-        term_ref[...] = total[...].astype(BF16)
-
-
-def mix(packed, both, down):
-    count, depth = packed.shape[0], packed.shape[1] - LANES
-    cols = both.shape[1]
+    total[...] = jnp.zeros_like(total)
+
+    def trip(j, _):
+        cols = pl.ds(pl.multiple_of(j * tile, tile), tile)
+        x = x_ref[:, :depth]
+        gate_act = jnp.dot(x, gate_ref[:, cols], preferred_element_type=F32)
+        up_act = jnp.dot(x, up_ref[:, cols], preferred_element_type=F32)
+        hidden = (gate_act / (1.0 + jnp.exp(-gate_act)) * up_act * scale).astype(BF16)
+        total[...] += jnp.dot(hidden, down_ref[cols, :], preferred_element_type=F32)
+        return 0
+
+    lax.fori_loop(0, gate_ref.shape[1] // tile, trip, 0)
+    term_ref[...] = total[...].astype(BF16)
+    for copy in copies:
+        copy.wait()
+
+
+def mix(packed, gate, up, down):
+    count = packed.shape[0]
+    cols = gate.shape[1]
     wide = down.shape[1]
     tile = next(w for w in (256, 128) if cols % w == 0)
-    whole = pl.BlockSpec((count, depth), lambda j: (0, 0))
-    column = pl.BlockSpec((depth, tile), lambda j: (0, j))
-    second = pl.BlockSpec((depth, tile), lambda j: (1, j))
-    row = pl.BlockSpec((tile, wide), lambda j: (j, 0))
+    vmem = pl.BlockSpec(memory_space=pltpu.VMEM)
+    hbm = pl.BlockSpec(memory_space=pl.ANY)
     return pl.pallas_call(
-        mix_kernel,
-        grid=(cols // tile,),
+        functools.partial(mix_kernel, tile),
         out_shape=(
-            jax.ShapeDtypeStruct((depth, cols), BF16),
-            jax.ShapeDtypeStruct((depth, cols), BF16),
+            jax.ShapeDtypeStruct(gate.shape, BF16),
+            jax.ShapeDtypeStruct(up.shape, BF16),
             jax.ShapeDtypeStruct(down.shape, BF16),
-            jax.ShapeDtypeStruct((count, wide), BF16),
+            pltpu.VMEM((count, wide), BF16),
         ),
-        in_specs=[whole, pl.BlockSpec((count, LANES), lambda j: (0, depth // LANES)), column, second, row],
-        out_specs=(column, column, row, pl.BlockSpec((count, wide), lambda j: (0, 0))),
-        scratch_shapes=[pltpu.VMEM((count, wide), F32)],
+        in_specs=[vmem] * 4,
+        out_specs=(hbm, hbm, hbm, vmem),
+        scratch_shapes=[pltpu.VMEM((count, wide), F32), pltpu.SemaphoreType.DMA((3,))],
         name="mix_tokens",
-        compiler_params=pltpu.CompilerParams(vmem_limit_bytes=48 << 20),
-    )(packed, packed, both, both, down)
+        compiler_params=pltpu.CompilerParams(vmem_limit_bytes=12 << 20),
+    )(packed, gate, up, down)
 
 
 def sum_kernel(n, term_ref, out_ref, near, near_in, far, far_in, last, last_in, s1, r1, s2, r2, s3, r3):
@@ -574,7 +576,7 @@
             dma((2, n)), dma((2, n)), dma((n,)), dma((n,)), dma((n,)), dma((n,)),
         ],
         name="sum_terms",
-        compiler_params=pltpu.CompilerParams(collective_id=1, has_side_effects=True),
+        compiler_params=pltpu.CompilerParams(collective_id=1, has_side_effects=True, vmem_limit_bytes=8 << 20),
     )(term)
 
 
@@ -593,8 +595,8 @@
 def body(mesh, tokens, routes, route_logits, gain, w_gate, w_up, w_down):
     n, depth = mesh.shape["fs"], tokens.shape[1]
     if fits(mesh, tokens, w_gate, w_down):
-        packed, both, down = move(mesh.shape["grp"], n, tokens, routes, route_logits, gain, w_gate, w_up, w_down)
-        gate, up, down, term = mix(packed, both, down)
+        packed, gate, up, down = move(mesh.shape["grp"], n, tokens, routes, route_logits, gain, w_gate, w_up, w_down)
+        gate, up, down, term = mix(packed, gate, up, down)
         return gate[None], up[None], down[None], sum_terms(n, term)
     values = tokens.astype(F32)
     mean_square = jnp.mean(values * values, axis=-1, keepdims=True)

time: 229 us -> 211 us (0.921)
  Pallas kernels: 225 us -> 210 us
  local copies, waits for them, and re-layouts: 3.68 us -> 0.63 us
    pallas_call x2, Pallas kernels: 205 us -> 192 us  [the longest x1 184 us: move(): pl.pallas_call(functools.partial(move_kernel, groups, n), out_shape=(pltp...]
    unnamed x5 -> x1, local copies, waits for them, and re-layouts: 3.68 us -> 0.63 us
where the time goes in v2:
time: 211 us
  Pallas kernels  210 us (100%)
    pallas_call x1, Pallas kernels, move(): pl.pallas_call(functools.partial(move_kernel, groups, n), out_shape=(pltp...  184 us
    pallas_call x1, Pallas kernels, sum_terms(): pl.pallas_call(functools.partial(sum_kernel, n), out_shape=jax.ShapeDtype...  17.8 us
    pallas_call x1, Pallas kernels, mix(): pl.pallas_call(functools.partial(mix_kernel, tile), out_shape=(jax.ShapeD...  7.91 us

profile of v2, /device:TPU:0, one launch (start us, length us, event | category | flops | bytes accessed | tf_op | source)
XLA Modules:
  0.0 211.1 jit_solution(6422815804547685137)
XLA Ops:
  0.6 184.0 %move_weights.1 = (bf16[256,2176]{1,0:T(8,128)(2,1)S(1)}, bf16[2048,1792]{1,0:T(8,128)(2,1)S(1)}, bf16[2048,1792]{1,0:T(8,128)(2,1)S(1)}, bf16[1792,2048]{1,0:T(8,128)(2,1)S(1)}) custom-call(bf16[64,2048]{1,0:T(8,128)(2,1)} %tokens_ref.1, s32[2,64]{1,0:T(2,128)} %bitcast.7, f32[2,64]{1,0:T(2,128)} %bitcast.8, f32[1,512]{1,0:T(1,128)} %bitcast.6, ...), custom_call_target="tpu_custom_call" | custom-call | tf_op jit(solution)/shard_map/move_weights/pallas_call | solution.py:389
  184.7 7.9 %mix_tokens.1 = (bf16[2048,1792]{1,0:T(8,128)(2,1)}, bf16[2048,1792]{1,0:T(8,128)(2,1)}, bf16[1792,2048]{1,0:T(8,128)(2,1)}, bf16[256,2048]{1,0:T(8,128)(2,1)S(1)}) custom-call(bf16[256,2176]{1,0:T(8,128)(2,1)S(1)} %get-tuple-element.12.x_ref, bf16[2048,1792]{1,0:T(8,128)(2,1)S(1)} %get-tuple-element.13.gate_ref, ...), custom_call_target="tpu_custom_call" | custom-call | tf_op jit(solution)/shard_map/mix_tokens/pallas_call | solution.py:475
  192.6 17.8 %sum_terms.1 = bf16[64,512]{1,0:T(8,128)(2,1)S(1)} custom-call(bf16[256,2048]{1,0:T(8,128)(2,1)S(1)} %get-tuple-element.19.term_ref), custom_call_target="tpu_custom_call" | custom-call | tf_op jit(solution)/shard_map/sum_terms/pallas_call | solution.py:564
  210.4 0.6 copy.12

commit v3 on v2

--- a/solution.py
+++ b/solution.py
@@ -9,17 +9,19 @@
 
 BF16 = jnp.bfloat16
 F32 = jnp.float32
-CHUNKS = 4
+CHUNKS = 8
 DOWN_CHUNKS = 4
-LOADS = 3
+LOADS = 4
 DOWN_LOADS = 2
-STEPS = 18
-OUTER_LEAD = 2
-OUTER_OWN = (0, 0, 1, 1, 2, 2, 3, 4, 6)
-OUTER_RELAY = (1, 1, 2, 2, 3, 3, 4, 5, 8)
-NEAR_LAG = 1
-IN_RATE, IN_LAG = 0.6, 1.0
-OUT_RATE, OUT_LAG = 0.5, 0.8
+AHEAD = 6
+DOWN_STEPS = (-3, 0, 4, 8)
+INNER_LEAD = 1
+OUTER_LEAD = 1
+FAR_RATE = 0.5
+SEND_RATE = 0.55
+NEAR_LAG = 2
+IN_LAG = 2
+OUT_LAG = 2.5
 LANES = 128
 
 
@@ -283,40 +285,44 @@
     inner = jnp.logical_not(outer)
     own_far = (t != near) & jnp.logical_not(home)
     send_tokens()
-    for i in range(items):
+    for c in range(DOWN_LOADS):
+        for k in order:
+            load_d(k, c).start()
+    sent = dict.fromkeys(("item", "inner own", "inner relay", "outer own", "outer relay", "near", "in", "out", "down"), 0)
+
+    def start_item(i):
         produce(i)
         own(i, t == near)
-        own(i, own_far & inner)
-        if i < OUTER_LEAD:
-            own(i, own_far & outer)
-        if i == 1:
-            for c in range(DOWN_LOADS):
-                for k in order:
-                    load_d(k, c).start()
-    sent = {"own": OUTER_LEAD, "relay": 0, "near": 0, "in": 0, "out": 0}
 
     def up_to(name, limit, act):
         while sent[name] < min(limit, items):
             act(sent[name])
             sent[name] += 1
 
-    for s in range(STEPS):
+    sent["down"] = items - DOWN_CHUNKS
+    s = 0
+    while min(sent.values()) < items:
+        paced = int(s * SEND_RATE)
+        up_to("item", s + AHEAD, start_item)
+        made = sent["item"]
+        up_to("inner own", min(made, INNER_LEAD + paced), lambda i: own(i, own_far & inner))
+        up_to("outer own", min(made, OUTER_LEAD + paced), lambda i: own(i, own_far & outer))
         if s < items:
             relay_home(s)
             relay_near(s)
-            relay_far(s, inner)
-        up_to("own", OUTER_LEAD + OUTER_OWN[min(s, len(OUTER_OWN) - 1)], lambda i: own(i, own_far & outer))
-        up_to("relay", OUTER_RELAY[min(s, len(OUTER_RELAY) - 1)], lambda i: relay_far(i, outer))
+        up_to("inner relay", min(s + 1, INNER_LEAD + paced), lambda i: relay_far(i, inner))
+        up_to("outer relay", min(s + 1, OUTER_LEAD + paced), lambda i: relay_far(i, outer))
         if s == 0:
             share_tokens()
-        if 1 <= s <= DOWN_CHUNKS:
-            down_step(s - 1)
         if s == items + 1:
             pair_tokens()
+        if s - items in DOWN_STEPS:
+            down_step(DOWN_STEPS.index(s - items))
+            sent["down"] += 1
         up_to("near", s + 1 - NEAR_LAG, lambda i: turn(near, i))
-        up_to("in", int((s + 1) * IN_RATE - IN_LAG), lambda i: turn(far[0], i))
-        up_to("out", int((s + 1) * OUT_RATE - OUT_LAG), lambda i: turn(far[1], i))
-        if s == items:
+        up_to("in", int((s + 1 - IN_LAG) * FAR_RATE), lambda i: turn(far[0], i))
+        up_to("out", int((s + 1 - OUT_LAG) * FAR_RATE), lambda i: turn(far[1], i))
+        if s == items + 2:
             @pl.when(home)
             def _():
                 for j in range(LOADS):
@@ -324,7 +330,7 @@
                         load(j, k, other_row).start()
                 for j in range(items):
                     home_step(j)
-    assert min(sent.values()) == items
+        s += 1
 
     def finish(i):
         @pl.when(home)

time: 211 us -> 205 us (0.972)
  Pallas kernels: 210 us -> 203 us
    pallas_call x1, Pallas kernels: 184 us -> 179 us  [move(): pl.pallas_call(functools.partial(move_kernel, groups, n), out_shape=(pltp...]
where the time goes in v3:
time: 205 us
  Pallas kernels  203 us (99%)
    pallas_call x1, Pallas kernels, move(): pl.pallas_call(functools.partial(move_kernel, groups, n), out_shape=(pltp...  179 us
    pallas_call x1, Pallas kernels, sum_terms(): pl.pallas_call(functools.partial(sum_kernel, n), out_shape=jax.ShapeDtype...  16.1 us
    pallas_call x1, Pallas kernels, mix(): pl.pallas_call(functools.partial(mix_kernel, tile), out_shape=(jax.ShapeD...  7.94 us

profile of v3, /device:TPU:0, one launch (start us, length us, event | category | flops | bytes accessed | tf_op | source)
XLA Modules:
  0.0 204.5 jit_solution(3198224596740656834)
XLA Ops:
  0.6 179.2 %move_weights.1 = (bf16[256,2176]{1,0:T(8,128)(2,1)S(1)}, bf16[2048,1792]{1,0:T(8,128)(2,1)S(1)}, bf16[2048,1792]{1,0:T(8,128)(2,1)S(1)}, bf16[1792,2048]{1,0:T(8,128)(2,1)S(1)}) custom-call(bf16[64,2048]{1,0:T(8,128)(2,1)} %tokens_ref.1, s32[2,64]{1,0:T(2,128)} %bitcast.7, f32[2,64]{1,0:T(2,128)} %bitcast.8, f32[1,512]{1,0:T(1,128)} %bitcast.6, ...), custom_call_target="tpu_custom_call" | custom-call | tf_op jit(solution)/shard_map/move_weights/pallas_call | solution.py:395
  179.9 7.9 %mix_tokens.1 = (bf16[2048,1792]{1,0:T(8,128)(2,1)}, bf16[2048,1792]{1,0:T(8,128)(2,1)}, bf16[1792,2048]{1,0:T(8,128)(2,1)}, bf16[256,2048]{1,0:T(8,128)(2,1)S(1)}) custom-call(bf16[256,2176]{1,0:T(8,128)(2,1)S(1)} %get-tuple-element.12.x_ref, bf16[2048,1792]{1,0:T(8,128)(2,1)S(1)} %get-tuple-element.13.gate_ref, ...), custom_call_target="tpu_custom_call" | custom-call | tf_op jit(solution)/shard_map/mix_tokens/pallas_call | solution.py:481
  187.8 16.1 %sum_terms.1 = bf16[64,512]{1,0:T(8,128)(2,1)S(1)} custom-call(bf16[256,2048]{1,0:T(8,128)(2,1)S(1)} %get-tuple-element.19.term_ref), custom_call_target="tpu_custom_call" | custom-call | tf_op jit(solution)/shard_map/sum_terms/pallas_call | solution.py:570
  203.9 0.6 copy.12

commit v4 on v3

--- a/solution.py
+++ b/solution.py
@@ -14,14 +14,14 @@
 LOADS = 4
 DOWN_LOADS = 2
 AHEAD = 6
-DOWN_STEPS = (-3, 0, 4, 8)
-INNER_LEAD = 1
+DOWN_STEPS = (-5, -2, 1, 4)
+INNER_LEAD = 2
 OUTER_LEAD = 1
 FAR_RATE = 0.5
-SEND_RATE = 0.55
+SEND_RATE = 0.5
 NEAR_LAG = 2
-IN_LAG = 2
-OUT_LAG = 2.5
+IN_LAG = 3
+OUT_LAG = 2
 LANES = 128
 
 
@@ -155,12 +155,26 @@
     def piece(source, q):
         return x_ref.at[pl.ds(pl.multiple_of(source * count + q * part, part), part), :]
 
-    def token_out(d):
+    def token_first(up):
         src = pack.at[pl.ds(pl.multiple_of(t * part, part), part), :]
-        return remote(src, piece(f, t), ts.at[d], tr.at[f], (g, lax.rem(f + d, n), t))
+        where = (g, f + 1, t) if up else (g, f - 1, t)
+        return remote(src, piece(f, t), ts.at[0 if up else 1, f], tr.at[f], where)
+
+    def token_on(source, up):
+        where = (g, f + 1, t) if up else (g, f - 1, t)
+        here = piece(source, t)
+        return remote(here, here, ts.at[0 if up else 1, source], tr.at[source], where)
+
+    def each_token(d, act):
+        for up in (True, False):
+            source = f - d if up else f + d
+
+            @pl.when((source >= 0) & (source < n))
+            def _():
+                act(source, up, (f + 1 < n) if up else (f > 0))
 
     def token_in(source):
-        return remote(piece(source, t), piece(source, t), ts.at[0], tr.at[source], (g, f, t))
+        return remote(piece(source, t), piece(source, t), ts.at[0, 0], tr.at[source], (g, f, t))
 
     def token_over(source):
         here = piece(source, t)
@@ -199,15 +213,27 @@
             table = jnp.where(lane == e, jnp.broadcast_to(column, (count, LANES)), table)
         pack[:, depth:] = table.astype(BF16)
         token_own().start()
-        for d in range(1, n):
-            token_out(d).start()
-
-    def share_tokens():
-        for d in range(1, n):
-            source = lax.rem(f + d, n)
+
+        @pl.when(f < n - 1)
+        def _():
+            token_first(True).start()
+
+        @pl.when(f > 0)
+        def _():
+            token_first(False).start()
+
+    def share_tokens(d):
+        def act(source, up, more):
             token_in(source).wait_recv()
+
+            @pl.when(more)
+            def _():
+                token_on(source, up).start()
+
             token_over(source).start()
             token_mate(source, 0).start()
+
+        each_token(d, act)
 
     def pair_tokens():
         for d in range(1, n):
@@ -273,13 +299,19 @@
                 load_d(k, c + DOWN_LOADS).start()
             down(k, c).start()
 
-    def home_step(i):
-        for k in (0, 1):
-            load(i, k, other_row).wait()
-            fold(i % LOADS, k, other_row(i % CHUNKS), extra.at[k, i])
-            if i + LOADS < items:
-                load(i + LOADS, k, other_row).start()
-            (extra_home if k == 0 else extra_mate)(i).start()
+    def start_extra(i):
+        @pl.when(home)
+        def _():
+            if i == 0:
+                for j in range(min(LOADS, items)):
+                    for k in (0, 1):
+                        load(j, k, other_row).start()
+            for k in (0, 1):
+                load(i, k, other_row).wait()
+                fold(i % LOADS, k, other_row(i % CHUNKS), extra.at[k, i])
+                if i + LOADS < items:
+                    load(i + LOADS, k, other_row).start()
+                (extra_home if k == 0 else extra_mate)(i).start()
 
     outer = (f == 0) | (f == n - 1)
     inner = jnp.logical_not(outer)
@@ -288,7 +320,7 @@
     for c in range(DOWN_LOADS):
         for k in order:
             load_d(k, c).start()
-    sent = dict.fromkeys(("item", "inner own", "inner relay", "outer own", "outer relay", "near", "in", "out", "down"), 0)
+    sent = dict.fromkeys(("item", "inner own", "inner relay", "outer own", "outer relay", "near", "in", "out", "down", "extra"), 0)
 
     def start_item(i):
         produce(i)
@@ -312,8 +344,8 @@
             relay_near(s)
         up_to("inner relay", min(s + 1, INNER_LEAD + paced), lambda i: relay_far(i, inner))
         up_to("outer relay", min(s + 1, OUTER_LEAD + paced), lambda i: relay_far(i, outer))
-        if s == 0:
-            share_tokens()
+        if s % 2 == 0 and s // 2 + 1 < n:
+            share_tokens(s // 2 + 1)
         if s == items + 1:
             pair_tokens()
         if s - items in DOWN_STEPS:
@@ -322,14 +354,8 @@
         up_to("near", s + 1 - NEAR_LAG, lambda i: turn(near, i))
         up_to("in", int((s + 1 - IN_LAG) * FAR_RATE), lambda i: turn(far[0], i))
         up_to("out", int((s + 1 - OUT_LAG) * FAR_RATE), lambda i: turn(far[1], i))
-        if s == items + 2:
-            @pl.when(home)
-            def _():
-                for j in range(LOADS):
-                    for k in (0, 1):
-                        load(j, k, other_row).start()
-                for j in range(items):
-                    home_step(j)
+        if made == items:
+            up_to("extra", sent["extra"] + 1, start_extra)
         s += 1
 
     def finish(i):
@@ -374,9 +400,24 @@
 
     lax.fori_loop(0, DOWN_CHUNKS, finish_d, 0)
     token_own().wait()
+
+    @pl.when(f < n - 1)
+    def _():
+        token_first(True).wait_send()
+
+    @pl.when(f > 0)
+    def _():
+        token_first(False).wait_send()
+
+    def sent_on(source, up, more):
+        @pl.when(more)
+        def _():
+            token_on(source, up).wait_send()
+
+    for d in range(1, n):
+        each_token(d, sent_on)
     for d in range(1, n):
         source = lax.rem(f + d, n)
-        token_out(d).wait_send()
         token_over(source).wait_send()
         for j in range(2):
             token_mate(source, j).wait_send()
@@ -428,7 +469,7 @@
             dma((n, items)),
             dma((n, DOWN_CHUNKS)),
             dma((n, DOWN_CHUNKS)),
-            dma((n,)),
+            dma((2, n)),
             dma((n,)),
             dma((n,)),
             dma((n,)),

time: 205 us -> 204 us (level)
    pallas_call x1, Pallas kernels: 179 us -> 176 us  [move(): pl.pallas_call(functools.partial(move_kernel, groups, n), out_shape=(pltp...]
where the time goes in v4:
time: 204 us; the launch traced here: 203 us
  Pallas kernels  202 us (99%)
    pallas_call x1, Pallas kernels, move(): pl.pallas_call(functools.partial(move_kernel, groups, n), out_shape=(pltp...  176 us
    pallas_call x1, Pallas kernels, sum_terms(): pl.pallas_call(functools.partial(sum_kernel, n), out_shape=jax.ShapeDtype...  18 us
    pallas_call x1, Pallas kernels, mix(): pl.pallas_call(functools.partial(mix_kernel, tile), out_shape=(jax.ShapeD...  7.94 us

profile of v4, /device:TPU:0, one launch (start us, length us, event | category | flops | bytes accessed | tf_op | source)
XLA Modules:
  0.0 203.4 jit_solution(18425121852831293037)
XLA Ops:
  0.6 176.2 %move_weights.1 = (bf16[256,2176]{1,0:T(8,128)(2,1)S(1)}, bf16[2048,1792]{1,0:T(8,128)(2,1)S(1)}, bf16[2048,1792]{1,0:T(8,128)(2,1)S(1)}, bf16[1792,2048]{1,0:T(8,128)(2,1)S(1)}) custom-call(bf16[64,2048]{1,0:T(8,128)(2,1)} %tokens_ref.1, s32[2,64]{1,0:T(2,128)} %bitcast.7, f32[2,64]{1,0:T(2,128)} %bitcast.8, f32[1,512]{1,0:T(1,128)} %bitcast.6, ...), custom_call_target="tpu_custom_call" | custom-call | tf_op jit(solution)/shard_map/move_weights/pallas_call | solution.py:436
  176.9 7.9 %mix_tokens.1 = (bf16[2048,1792]{1,0:T(8,128)(2,1)}, bf16[2048,1792]{1,0:T(8,128)(2,1)}, bf16[1792,2048]{1,0:T(8,128)(2,1)}, bf16[256,2048]{1,0:T(8,128)(2,1)S(1)}) custom-call(bf16[256,2176]{1,0:T(8,128)(2,1)S(1)} %get-tuple-element.12.x_ref, bf16[2048,1792]{1,0:T(8,128)(2,1)S(1)} %get-tuple-element.13.gate_ref, ...), custom_call_target="tpu_custom_call" | custom-call | tf_op jit(solution)/shard_map/mix_tokens/pallas_call | solution.py:522
  184.8 18.0 %sum_terms.1 = bf16[64,512]{1,0:T(8,128)(2,1)S(1)} custom-call(bf16[256,2048]{1,0:T(8,128)(2,1)S(1)} %get-tuple-element.19.term_ref), custom_call_target="tpu_custom_call" | custom-call | tf_op jit(solution)/shard_map/sum_terms/pallas_call | solution.py:611
  202.8 0.6 copy.12
